TPU v7x, 32 devices: a whole 2x2x4 slice. The times are simulated.
32 devices in a mesh: dp: 4 (over y, x), kv: 4 (over z), tp: 2 (over core).
Axes of the slice: x: 2, y: 2, z: 4, core: 2. Of those that a mesh axis runs over, the one named last changes fastest.
Arguments:
- tokens: bfloat16 [16, 4096], P('dp', 'kv'), may hold values from -24 to 24
- positions: int32 [16], P(('dp', 'kv')), may hold values from 0 to 4095
- state: float32 [16, 16, 128, 128], P(('dp', 'kv'), 'tp'), may hold values from -0.6 to 0.6
- w_query: bfloat16 [4096, 2048], P('kv', 'tp'), may hold values from -0.09375 to 0.09375
- w_key: bfloat16 [4096, 2048], P('kv', 'tp'), may hold values from -0.09375 to 0.09375
- w_value: bfloat16 [4096, 2048], P('kv', 'tp'), may hold values from -0.09375 to 0.09375
- w_gate: bfloat16 [4096, 2048], P('kv', 'tp'), may hold values from -0.09375 to 0.09375
- w_out: bfloat16 [2048, 4096], P(None, ('kv', 'tp')), may hold values from -0.25 to 0.25
- gain_mix: float32 [4096], replicated, may hold values from 0.1 to 1.9
- w_ffn_gate: bfloat16 [4096, 11008], P(None, ('kv', 'tp')), may hold values from -0.09375 to 0.09375
- w_ffn_up: bfloat16 [4096, 11008], P(None, ('kv', 'tp')), may hold values from -0.09375 to 0.09375
- w_ffn_down: bfloat16 [11008, 4096], P(('kv', 'tp')), may hold values from -0.109375 to 0.109375
- gain_out: float32 [4096], replicated, may hold values from 0.1 to 1.9
Outputs:
- layer_out: bfloat16 [16, 4096], P('dp', ('kv', 'tp'))
- new_state: float32 [16, 16, 128, 128], P(('dp', 'kv'), 'tp')
All inputs are finite; a program needn't handle non-finite values.
Results may differ from a plain program's by a relative error of at most 0.018.
Values may be sent and summed in bfloat16 or wider, within the bound.
A program may use at most 128 MiB of HBM per device.

v0:
```python
import functools

import jax
import jax.numpy as jnp
import numpy as np
from jax import lax
from jax.experimental import pallas as pl
from jax.experimental.pallas import tpu as pltpu
from jax.sharding import PartitionSpec as P

MESH = pl.DeviceIdType.MESH
F32 = jnp.float32
BF16 = jnp.bfloat16


def dot_rows(values, weight):
    return lax.dot_general(values, weight, (((1,), (1,)), ((), ())), preferred_element_type=F32)


def step_kernel(
    kv_count,
    tp_count,
    tok_h,
    pos_h,
    state_h,
    wq_h,
    wk_h,
    wv_h,
    wg_h,
    wout_h,
    gmix_h,
    wfg_h,
    wfu_h,
    wfd_h,
    gout_h,
    inv_h,
    out_v,
    nst,
    tok,
    pos,
    state,
    wq,
    wk,
    wv,
    wg,
    wout,
    gmix,
    wfg,
    wfu,
    wfd,
    gout,
    inv,
    qsend,
    qrecv,
    att,
    mix,
    hid_own,
    hid,
    inner,
    fsend,
    frecv,
    sums,
    local_sem,
    q_send_sem,
    q_recv_sem,
    send_sem,
    recv_sem,
):
    group = kv_count * tp_count
    dp = lax.axis_index("dp")
    kv = lax.axis_index("kv")
    tp = lax.axis_index("tp")
    me = kv * tp_count + tp
    rows = tok.shape[0]
    heads = state.shape[0]
    width_head = state.shape[1]
    width = hid.shape[1]
    cols = mix.shape[2]
    ff = wfg.shape[0]

    far = sorted(range(1, kv_count), key=lambda d: -min(d, kv_count - d))
    steps = [(d, e) for d in far for e in range(tp_count)]
    steps += [(0, e) for e in range(1, tp_count)]

    def partner(d, e):
        return lax.rem(kv + d, kv_count), lax.rem(tp + e, tp_count)

    barrier = pltpu.get_barrier_semaphore()
    for d, e in steps:
        other_kv, other_tp = partner(d, e)
        pl.semaphore_signal(
            barrier, inc=1, device_id=(dp, other_kv, other_tp), device_id_type=MESH
        )

    loads = []

    def load(src, dst):
        copy = pltpu.make_async_copy(src, dst, local_sem.at[len(loads)])
        copy.start()
        loads.append(copy)
        return copy

    tok_load = load(tok_h, tok)
    pos_load = load(pos_h, pos)
    inv_load = load(inv_h, inv)
    proj_loads = [
        load(src, dst) for src, dst in ((wq_h, wq), (wk_h, wk), (wv_h, wv), (wg_h, wg))
    ]
    state_load = load(state_h, state)
    gmix_load = load(gmix_h, gmix)
    gout_load = load(gout_h, gout)

    pos_load.wait()
    inv_load.wait()
    lane = lax.broadcasted_iota(jnp.int32, (1, width_head), 1)
    angle = pos[...].astype(F32) * inv[...]
    cosine = jnp.cos(angle)
    sine = jnp.sin(angle)
    sine = jnp.where(lane < width_head // 2, -sine, sine)

    tok_load.wait()
    pl.semaphore_wait(barrier, group - 1)
    later = []
    q_copies = []
    for p, weight in enumerate((wq, wk, wv, wg)):
        proj_loads[p].wait()
        if p == 0:
            later.append(load(wout_h, wout))
        elif p == 1:
            later.append(load(wfg_h, wfg))
        elif p == 2:
            later.append(load(wfu_h, wfu))
        else:
            later.append(load(wfd_h, wfd))
        part = jnp.dot(tok[...], weight[...], preferred_element_type=F32)
        for i in range(kv_count):
            for h in range(heads):
                qsend[i, p, h : h + 1, :] = part[
                    i : i + 1, h * width_head : (h + 1) * width_head
                ]
        for d in far:
            other_kv, _ = partner(d, 0)
            copy = pltpu.make_async_remote_copy(
                src_ref=qsend.at[other_kv, p],
                dst_ref=qrecv.at[kv, p],
                send_sem=q_send_sem.at[p, d],
                recv_sem=q_recv_sem.at[p, d],
                device_id=(dp, other_kv, tp),
                device_id_type=MESH,
            )
            copy.start()
            q_copies.append((p, d, copy))
    wout_load, wfg_load, wfu_load, wfd_load = later

    head_id = (tp * heads + lax.broadcasted_iota(jnp.int32, (heads, width_head), 0)).astype(F32)
    total_heads = heads * tp_count
    decay = 1.0 - jnp.exp2(-5.0 - 6.0 * head_id / (total_heads - 1))

    def rotate_row(x):
        return x * cosine + pltpu.roll(x, width_head // 2, 1) * sine

    projected = []
    for p in range(4):
        total = qsend[kv, p]
        for q, d, copy in q_copies:
            if q == p:
                copy.wait_recv()
                total = total + qrecv[lax.rem(kv + kv_count - d, kv_count), p]
        projected.append(total)
    query, key, value, gate_pre = projected
    query = rotate_row(query)
    key = rotate_row(key) * width_head ** (-0.5)
    query_t = jnp.transpose(query)
    key_t = jnp.transpose(key)
    state_load.wait()
    retained = []
    for h in range(heads):
        new = decay[h : h + 1, :] * state[h] + key_t[:, h : h + 1] * value[h : h + 1, :]
        nst[h] = new
        retained.append(jnp.sum(query_t[:, h : h + 1] * new, axis=0, keepdims=True))
    retained = jnp.concatenate(retained, axis=0)
    mean = jnp.mean(retained, -1, keepdims=True)
    var = jnp.mean(jnp.square(retained - mean), -1, keepdims=True)
    normed = (retained - mean) * lax.rsqrt(var + 1e-05)
    silu_gate = gate_pre / (1.0 + jnp.exp(-gate_pre))
    attended = (normed * silu_gate).astype(BF16).astype(F32)
    own_rows = pl.ds(pl.multiple_of(me * heads, heads), heads)
    att[own_rows, :] = attended

    def send_all(phase, src, dst):
        copies = []
        for d, e in steps:
            other_kv, other_tp = partner(d, e)
            copy = pltpu.make_async_remote_copy(
                src_ref=src,
                dst_ref=dst,
                send_sem=send_sem.at[phase, d * tp_count + e],
                recv_sem=recv_sem.at[phase, d * tp_count + e],
                device_id=(dp, other_kv, other_tp),
                device_id_type=MESH,
            )
            copy.start()
            copies.append(copy)
        return copies

    att_copies = send_all(0, att.at[own_rows, :], att.at[own_rows, :])

    wout_load.wait()
    for copy in att_copies:
        copy.wait_recv()
    lhs = jnp.concatenate(
        [
            att[pl.ds(t * heads + h, rows, stride=tp_count * heads), :]
            for t in range(tp_count)
            for h in range(heads)
        ],
        axis=1,
    ).astype(BF16)
    mixed = jnp.dot(lhs, wout[...], preferred_element_type=F32)
    tok_own = tok[:, pl.ds(pl.multiple_of(tp * cols, cols), cols)]
    mix[me] = (tok_own.astype(F32) + mixed).astype(BF16)
    mix_copies = send_all(1, mix.at[me], mix.at[me])
    gmix_load.wait()
    gout_load.wait()
    for copy in mix_copies:
        copy.wait_recv()
    whole = [mix[p].astype(F32) for p in range(group)]
    total = functools.reduce(lambda a, b: a + b, whole)
    squares = functools.reduce(lambda a, b: a + b, [x * x for x in whole])
    mean = jnp.sum(total, 1, keepdims=True) / width
    var = jnp.sum(squares, 1, keepdims=True) / width - mean * mean
    scale = lax.rsqrt(var + 1e-05)
    for p in range(group):
        block = slice(p * cols, (p + 1) * cols)
        hidden = ((whole[p] - mean) * scale * gmix[:, block]).astype(BF16)
        hid[:, block] = hidden
        hid_own[p] = hidden.astype(F32)

    wfg_load.wait()
    wfu_load.wait()
    tile = 256
    whole_tiles = ff // tile

    def inner_block(at):
        gate = dot_rows(hid[...], wfg[at, :])
        upward = dot_rows(hid[...], wfu[at, :])
        inner[:, at] = (gate / (1.0 + jnp.exp(-gate)) * upward).astype(BF16)

    for j in range(whole_tiles):
        inner_block(pl.ds(j * tile, tile))

    if ff % tile:
        inner_block(pl.ds(whole_tiles * tile, ff % tile))

    wfd_load.wait()
    main = ff // 128 * 128

    def down_block(owner):
        at = pl.ds(pl.multiple_of(owner * cols, cols), cols)
        result = jnp.dot(inner[:, :main], wfd[:main, at], preferred_element_type=F32)
        if main < ff:
            result += jnp.dot(inner[:, main:], wfd[main:, at], preferred_element_type=F32)
        return result

    f_copies = []
    for d, e in steps:
        other_kv, other_tp = partner(d, e)
        owner = other_kv * tp_count + other_tp
        fsend[owner] = down_block(owner).astype(BF16)
        copy = pltpu.make_async_remote_copy(
            src_ref=fsend.at[owner],
            dst_ref=frecv.at[me],
            send_sem=send_sem.at[2, d * tp_count + e],
            recv_sem=recv_sem.at[2, d * tp_count + e],
            device_id=(dp, other_kv, other_tp),
            device_id_type=MESH,
        )
        copy.start()
        f_copies.append((d, e, copy))
    summed = hid_own[me] + down_block(me)
    for d, e, copy in f_copies:
        copy.wait_recv()
        source = lax.rem(kv + kv_count - d, kv_count) * tp_count + lax.rem(
            tp + tp_count - e, tp_count
        )
        summed = summed + frecv[source].astype(F32)
    own_sum = jnp.sum(summed, 1, keepdims=True)
    own_square = jnp.sum(summed * summed, 1, keepdims=True)
    low_half = lax.broadcasted_iota(jnp.int32, (rows, 128), 1) < 64
    sums[me] = jnp.where(low_half, own_sum, own_square)
    sum_copies = send_all(3, sums.at[me], sums.at[me])
    for copy in sum_copies:
        copy.wait_recv()
    all_sums = functools.reduce(lambda a, b: a + b, [sums[p] for p in range(group)])
    mean = all_sums[:, :1] / width
    var = all_sums[:, 64:65] / width - mean * mean
    gain = gout[:, pl.ds(pl.multiple_of(me * cols, cols), cols)]
    out_v[...] = ((summed - mean) * lax.rsqrt(var + 1e-05) * gain).astype(BF16)

    for _, _, copy in q_copies:
        copy.wait_send()
    for copies in (att_copies, mix_copies, sum_copies):
        for copy in copies:
            copy.wait_send()
    for _, _, copy in f_copies:
        copy.wait_send()


def store_kernel(out_v, nst_v, out_h, nst_h, sem):
    copies = [
        pltpu.make_async_copy(nst_v, nst_h, sem.at[0]),
        pltpu.make_async_copy(out_v, out_h, sem.at[1]),
    ]
    for copy in copies:
        copy.start()
    for copy in copies:
        copy.wait()


def fused_step(
    tokens,
    positions,
    state,
    w_query,
    w_key,
    w_value,
    w_gate,
    w_out,
    gain_mix,
    w_ffn_gate,
    w_ffn_up,
    w_ffn_down,
    gain_out,
):
    kv_count = lax.axis_size("kv")
    tp_count = lax.axis_size("tp")
    group = kv_count * tp_count
    rows = tokens.shape[0]
    _, heads, width_head, _ = state.shape
    width = w_ffn_gate.shape[0]
    cols = w_out.shape[1]
    half = width_head // 2
    inverse = 10000.0 ** (-np.arange(half, dtype=np.float32) / half)
    inverse = np.tile(inverse.astype(np.float32), 2)[None, :]
    arrays = (
        tokens,
        positions[None, :],
        state[0],
        w_query,
        w_key,
        w_value,
        w_gate,
        w_out,
        gain_mix[None, :],
        w_ffn_gate.T,
        w_ffn_up.T,
        w_ffn_down,
        gain_out[None, :],
        jnp.asarray(inverse),
    )
    held = [pltpu.VMEM(a.shape, a.dtype) for a in arrays]
    vmem_spec = pl.BlockSpec(memory_space=pltpu.VMEM)
    any_spec = pl.BlockSpec(memory_space=pl.ANY)
    out, new_state = pl.pallas_call(
        functools.partial(step_kernel, kv_count, tp_count),
        out_shape=(
            pltpu.VMEM((rows, cols), BF16),
            pltpu.VMEM(state.shape[1:], F32),
        ),
        in_specs=[any_spec] * len(arrays),
        out_specs=(vmem_spec, vmem_spec),
        scratch_shapes=held
        + [
            pltpu.VMEM((kv_count, 4, heads, width_head), F32),
            pltpu.VMEM((kv_count, 4, heads, width_head), F32),
            pltpu.VMEM((group * heads, width_head), F32),
            pltpu.VMEM((group, rows, cols), BF16),
            pltpu.VMEM((group, rows, cols), F32),
            pltpu.VMEM((rows, width), BF16),
            pltpu.VMEM((rows, w_ffn_gate.shape[1]), BF16),
            pltpu.VMEM((group, rows, cols), BF16),
            pltpu.VMEM((group, rows, cols), BF16),
            pltpu.VMEM((group, rows, 128), F32),
            pltpu.SemaphoreType.DMA((len(arrays) + 1,)),
            pltpu.SemaphoreType.DMA((4, kv_count)),
            pltpu.SemaphoreType.DMA((4, kv_count)),
            pltpu.SemaphoreType.DMA((4, group)),
            pltpu.SemaphoreType.DMA((4, group)),
        ],
        compiler_params=pltpu.CompilerParams(
            collective_id=0, has_side_effects=True, vmem_limit_bytes=56 * 2**20
        ),
    )(*arrays)
    out, new_state = pl.pallas_call(
        store_kernel,
        out_shape=(
            jax.ShapeDtypeStruct(out.shape, out.dtype),
            jax.ShapeDtypeStruct(new_state.shape, new_state.dtype),
        ),
        in_specs=[vmem_spec, vmem_spec],
        out_specs=(any_spec, any_spec),
        scratch_shapes=[pltpu.SemaphoreType.DMA((2,))],
        compiler_params=pltpu.CompilerParams(vmem_limit_bytes=2**20),
    )(out, new_state)
    return out, new_state[None]


def fits_kernel(tokens, state, w_out, kv_count, tp_count):
    seqs, _, width_head, _ = state.shape
    return (
        seqs == 1
        and width_head == 128
        and w_out.shape[1] % 128 == 0
        and tokens.shape[0] == kv_count
        and kv_count * tp_count <= 16
    )


def rotate(vectors, positions):
    half = vectors.shape[-1] // 2
    inverse = 10000.0 ** (-jnp.arange(half, dtype=jnp.float32) / half)
    angle = positions.astype(jnp.float32)[:, None, None] * inverse[None, None, :]
    cosine = jnp.cos(angle)
    sine = jnp.sin(angle)
    first = vectors[..., :half]
    second = vectors[..., half:]
    return jnp.concatenate([first * cosine - second * sine, first * sine + second * cosine], -1)


def finish_norm(values, sums, squares, count, gain):
    mean = sums / count
    var = squares / count - mean * mean
    return (values - mean[:, None]) * lax.rsqrt(var + 1e-05)[:, None] * gain[None, :]


def on_device(
    tokens,
    positions,
    state,
    w_query,
    w_key,
    w_value,
    w_gate,
    w_out,
    gain_mix,
    w_ffn_gate,
    w_ffn_up,
    w_ffn_down,
    gain_out,
):
    if fits_kernel(tokens, state, w_out, lax.axis_size("kv"), lax.axis_size("tp")):
        return fused_step(
            tokens,
            positions,
            state,
            w_query,
            w_key,
            w_value,
            w_gate,
            w_out,
            gain_mix,
            w_ffn_gate,
            w_ffn_up,
            w_ffn_down,
            gain_out,
        )
    seqs = state.shape[0]
    heads = state.shape[1]
    width_head = state.shape[2]
    proj_cols = w_query.shape[1]
    width = w_ffn_gate.shape[0]
    cols = w_out.shape[1]
    group_rows = tokens.shape[0]
    kv_count = lax.axis_size("kv")
    tp_count = lax.axis_size("tp")
    tp_index = lax.axis_index("tp")
    col_start = (lax.axis_index("kv") * tp_count + tp_index) * cols
    projected = lax.psum_scatter(
        jnp.concatenate(
            [
                jnp.dot(tokens, w_query, preferred_element_type=jnp.float32),
                jnp.dot(tokens, w_key, preferred_element_type=jnp.float32),
                jnp.dot(tokens, w_value, preferred_element_type=jnp.float32),
                jnp.dot(tokens, w_gate, preferred_element_type=jnp.float32),
            ],
            axis=1,
        ),
        "kv",
        scatter_dimension=0,
        tiled=True,
    )
    query = projected[:, :proj_cols].reshape(seqs, heads, width_head)
    key = projected[:, proj_cols : 2 * proj_cols].reshape(seqs, heads, width_head)
    value = projected[:, 2 * proj_cols : 3 * proj_cols].reshape(seqs, heads, width_head)
    gate_pre = projected[:, 3 * proj_cols :]
    query = rotate(query, positions)
    key = rotate(key, positions) * width_head ** (-0.5)
    total_heads = heads * tp_count
    head_ids = (tp_index * heads + jnp.arange(heads, dtype=jnp.int32)).astype(jnp.float32)
    decay = 1.0 - 2.0 ** (-5.0 - 6.0 * head_ids / (total_heads - 1))
    new_state = decay[None, :, None, None] * state + key[:, :, :, None] * value[:, :, None, :]
    retained = jnp.einsum("bhd,bhdv->bhv", query, new_state, precision=lax.Precision.HIGHEST)
    mean = jnp.mean(retained, -1, keepdims=True)
    var = jnp.mean(jnp.square(retained - mean), -1, keepdims=True)
    normed = (retained - mean) * lax.rsqrt(var + 1e-05)
    attended = (normed.reshape(seqs, proj_cols) * jax.nn.silu(gate_pre)).astype(jnp.bfloat16)
    gathered = lax.all_gather(attended[None], ("kv", "tp"), axis=0, tiled=True)
    gathered = gathered.reshape(kv_count, tp_count, seqs, proj_cols)
    out_blocks = w_out.reshape(tp_count, proj_cols, cols)
    mixed = jnp.einsum(
        "itsc,tcd->isd", gathered, out_blocks, preferred_element_type=jnp.float32
    ).reshape(group_rows, cols)
    tokens_own = lax.dynamic_slice_in_dim(tokens, tp_index * cols, cols, 1)
    mixed_pre = (tokens_own.astype(jnp.float32) + mixed).astype(jnp.bfloat16)
    gain_out_own = lax.dynamic_slice_in_dim(gain_out, col_start, cols, 0)
    whole_rows = lax.all_gather(mixed_pre, ("kv", "tp"), axis=1, tiled=True).astype(jnp.float32)
    hidden = finish_norm(
        whole_rows, jnp.sum(whole_rows, 1), jnp.sum(whole_rows * whole_rows, 1), width, gain_mix
    ).astype(jnp.bfloat16)
    hidden_own = lax.dynamic_slice_in_dim(hidden, col_start, cols, 1)
    gate = jnp.dot(hidden, w_ffn_gate, preferred_element_type=jnp.float32)
    upward = jnp.dot(hidden, w_ffn_up, preferred_element_type=jnp.float32)
    inner = (jax.nn.silu(gate) * upward).astype(jnp.bfloat16)
    ffn_cols = lax.psum_scatter(
        lax.dot_general(
            w_ffn_down, inner, (((0,), (1,)), ((), ())), preferred_element_type=jnp.float32
        ),
        ("kv", "tp"),
        scatter_dimension=0,
        tiled=True,
    )
    summed = hidden_own.astype(jnp.float32) + ffn_cols.T
    out_sums, out_squares = lax.psum(
        (jnp.sum(summed, 1), jnp.sum(summed * summed, 1)), ("kv", "tp")
    )
    layer_out = finish_norm(summed, out_sums, out_squares, width, gain_out_own).astype(jnp.bfloat16)
    return (layer_out, new_state)


def solution(mesh):
    return jax.shard_map(
        on_device,
        mesh=mesh,
        in_specs=(
            P("dp", "kv"),
            P(("dp", "kv")),
            P(("dp", "kv"), "tp", None, None),
            P("kv", "tp"),
            P("kv", "tp"),
            P("kv", "tp"),
            P("kv", "tp"),
            P(None, ("kv", "tp")),
            P(),
            P(None, ("kv", "tp")),
            P(None, ("kv", "tp")),
            P(("kv", "tp"), None),
            P(),
        ),
        out_specs=(P("dp", ("kv", "tp")), P(("dp", "kv"), "tp", None, None)),
        check_vma=False,
    )
```

profile of v0, /device:TPU:0, one launch (start us, length us, event | category | flops | bytes accessed | tf_op | source)
XLA Modules:
  0.0 37.1 jit_solution(12187359945655810571)
XLA Ops:
  1.3 35.0 %shard_map.149 = (bf16[4,512]{1,0:T(4,128)(2,1)S(1)}, f32[8,128,128]{2,1,0:T(8,128)S(1)}) custom-call(bf16[4,1024]{1,0:T(4,128)(2,1)} %tok_h.1, s32[1,1]{1,0:T(1,128)} %bitcast.7.pos_h, f32[8,128,128]{2,1,0:T(8,128)} %bitcast.10, bf16[1024,1024]{1,0:T(8,128)(2,1)} %wq_h.1, bf16[1024,1024]{1,0:T(8,128)(2,1)} %wk_h.1, bf16[1024,1024]{1,0:T(8,128)(2,1)} %wv_h.1, ...), custom_call_target="tpu_custom_call" | custom-call | tf_op jit(solution)/shard_map/pallas_call | solution.py:364
  36.3 0.8 %shard_map.150 = (bf16[4,512]{1,0:T(4,128)(2,1)}, f32[8,128,128]{2,1,0:T(8,128)}) custom-call(bf16[4,512]{1,0:T(4,128)(2,1)S(1)} %get-tuple-element.6.out_v, f32[8,128,128]{2,1,0:T(8,128)S(1)} %get-tuple-element.7.nst_v), custom_call_target="tpu_custom_call" | custom-call | tf_op jit(solution)/shard_map/pallas_call | solution.py:394
where the time goes:
time: 37.3 us; the launch traced here: 37.1 us
  Pallas kernels  35.8 us (96%)
  between operations  1.29 us (3%)
    pallas_call x1, Pallas kernels, fused_step(): pl.pallas_call(functools.partial(step_kernel, kv_count, tp_count), out_sh...  35 us
    pallas_call x1, Pallas kernels, fused_step(): pl.pallas_call(store_kernel, out_shape=(jax.ShapeDtypeStruct(out.shape, o...  0.81 us

commit v1 on v0

--- a/solution.py
+++ b/solution.py
@@ -17,7 +17,38 @@
     return lax.dot_general(values, weight, (((1,), (1,)), ((), ())), preferred_element_type=F32)
 
 
-def step_kernel(
+def near_first(kv, count):
+    low = jnp.minimum(kv, count - 1 - kv)
+    step = jnp.where(2 * kv < count, 1, -1)
+    order = []
+    for k in range(1, count):
+        offset = jnp.where(
+            k <= 2 * low, (k + 1) // 2 * (1 if k % 2 == 0 else -1), (k - low) * step
+        )
+        order.append(kv + offset)
+    return order
+
+
+def step_kernel(kv_count, tp_count, *refs):
+    operands = 14
+
+    def body(local_sem, q_send_sem, q_recv_sem, send_sem, recv_sem):
+        step_body(
+            kv_count, tp_count, *refs, local_sem, q_send_sem, q_recv_sem, send_sem, recv_sem
+        )
+
+    group = kv_count * tp_count
+    pl.run_scoped(
+        body,
+        pltpu.SemaphoreType.DMA((operands,)),
+        pltpu.SemaphoreType.DMA((4, kv_count)),
+        pltpu.SemaphoreType.DMA((4, kv_count)),
+        pltpu.SemaphoreType.DMA((4, group)),
+        pltpu.SemaphoreType.DMA((4, group)),
+    )
+
+
+def step_body(
     kv_count,
     tp_count,
     tok_h,
@@ -53,9 +84,11 @@
     qsend,
     qrecv,
     att,
+    att_rows,
     mix,
-    hid_own,
-    hid,
+    gain_rows,
+    acc_gate,
+    acc_up,
     inner,
     fsend,
     frecv,
@@ -74,23 +107,19 @@
     rows = tok.shape[0]
     heads = state.shape[0]
     width_head = state.shape[1]
-    width = hid.shape[1]
+    width = wfg.shape[1]
     cols = mix.shape[2]
     ff = wfg.shape[0]
 
-    far = sorted(range(1, kv_count), key=lambda d: -min(d, kv_count - d))
-    steps = [(d, e) for d in far for e in range(tp_count)]
-    steps += [(0, e) for e in range(1, tp_count)]
-
-    def partner(d, e):
-        return lax.rem(kv + d, kv_count), lax.rem(tp + e, tp_count)
+    near = near_first(kv, kv_count)
+    beside = [lax.rem(tp + e, tp_count) for e in range(1, tp_count)]
+    far_peers = [(chip, core) for chip in reversed(near) for core in range(tp_count)]
+    near_peers = [(kv, core) for core in beside]
+    near_peers += [(chip, core) for chip in near for core in range(tp_count)]
 
     barrier = pltpu.get_barrier_semaphore()
-    for d, e in steps:
-        other_kv, other_tp = partner(d, e)
-        pl.semaphore_signal(
-            barrier, inc=1, device_id=(dp, other_kv, other_tp), device_id_type=MESH
-        )
+    for chip, core in far_peers + [(kv, core) for core in beside]:
+        pl.semaphore_signal(barrier, inc=1, device_id=(dp, chip, core), device_id_type=MESH)
 
     loads = []
 
@@ -119,98 +148,134 @@
     sine = jnp.where(lane < width_head // 2, -sine, sine)
 
     tok_load.wait()
-    pl.semaphore_wait(barrier, group - 1)
     later = []
     q_copies = []
+
+    def send_part(p):
+        for d in range(kv_count - 1, 0, -1):
+            chip = near[d - 1]
+            copy = pltpu.make_async_remote_copy(
+                src_ref=qsend.at[chip, p],
+                dst_ref=qrecv.at[kv, p],
+                send_sem=q_send_sem.at[p, d],
+                recv_sem=q_recv_sem.at[p, kv],
+                device_id=(dp, chip, tp),
+                device_id_type=MESH,
+            )
+            copy.start()
+            q_copies.append(copy)
+
+    following = ((wout_h, wout), (wfg_h, wfg), (wfu_h, wfu), (wfd_h, wfd))
     for p, weight in enumerate((wq, wk, wv, wg)):
         proj_loads[p].wait()
-        if p == 0:
-            later.append(load(wout_h, wout))
-        elif p == 1:
-            later.append(load(wfg_h, wfg))
-        elif p == 2:
-            later.append(load(wfu_h, wfu))
-        else:
-            later.append(load(wfd_h, wfd))
+        later.append(load(*following[p]))
         part = jnp.dot(tok[...], weight[...], preferred_element_type=F32)
         for i in range(kv_count):
             for h in range(heads):
                 qsend[i, p, h : h + 1, :] = part[
                     i : i + 1, h * width_head : (h + 1) * width_head
                 ]
-        for d in far:
-            other_kv, _ = partner(d, 0)
-            copy = pltpu.make_async_remote_copy(
-                src_ref=qsend.at[other_kv, p],
-                dst_ref=qrecv.at[kv, p],
-                send_sem=q_send_sem.at[p, d],
-                recv_sem=q_recv_sem.at[p, d],
-                device_id=(dp, other_kv, tp),
-                device_id_type=MESH,
-            )
-            copy.start()
-            q_copies.append((p, d, copy))
+        if p == 2:
+            pl.semaphore_wait(barrier, group - 1)
+            for done in range(3):
+                send_part(done)
+        elif p == 3:
+            send_part(p)
     wout_load, wfg_load, wfu_load, wfd_load = later
 
     head_id = (tp * heads + lax.broadcasted_iota(jnp.int32, (heads, width_head), 0)).astype(F32)
     total_heads = heads * tp_count
     decay = 1.0 - jnp.exp2(-5.0 - 6.0 * head_id / (total_heads - 1))
 
+    gmix_load.wait()
+    gain = gmix[...]
+    gain_high = gain.astype(BF16).astype(F32)
+    row_id = lax.broadcasted_iota(jnp.int32, (8, width), 0)
+    gain_rows[...] = jnp.where(
+        row_id == rows, gain_high, jnp.where(row_id == rows + 1, gain - gain_high, 0.0)
+    )
+
     def rotate_row(x):
         return x * cosine + pltpu.roll(x, width_head // 2, 1) * sine
 
-    projected = []
-    for p in range(4):
+    def collect(p):
         total = qsend[kv, p]
-        for q, d, copy in q_copies:
-            if q == p:
-                copy.wait_recv()
-                total = total + qrecv[lax.rem(kv + kv_count - d, kv_count), p]
-        projected.append(total)
-    query, key, value, gate_pre = projected
-    query = rotate_row(query)
-    key = rotate_row(key) * width_head ** (-0.5)
+        for chip in near:
+            pltpu.make_async_remote_copy(
+                src_ref=qsend.at[chip, p],
+                dst_ref=qrecv.at[chip, p],
+                send_sem=q_send_sem.at[p, 0],
+                recv_sem=q_recv_sem.at[p, chip],
+                device_id=(dp, chip, tp),
+                device_id_type=MESH,
+            ).wait_recv()
+            total = total + qrecv[chip, p]
+        return total
+
+    state_load.wait()
+    query = rotate_row(collect(0))
     query_t = jnp.transpose(query)
-    key_t = jnp.transpose(key)
-    state_load.wait()
-    retained = []
-    for h in range(heads):
-        new = decay[h : h + 1, :] * state[h] + key_t[:, h : h + 1] * value[h : h + 1, :]
-        nst[h] = new
-        retained.append(jnp.sum(query_t[:, h : h + 1] * new, axis=0, keepdims=True))
-    retained = jnp.concatenate(retained, axis=0)
+    held = jnp.concatenate(
+        [
+            jnp.sum(query_t[:, h : h + 1] * state[h], axis=0, keepdims=True)
+            for h in range(heads)
+        ],
+        axis=0,
+    )
+    key = rotate_row(collect(1)) * width_head ** (-0.5)
+    match = jnp.sum(query * key, axis=1, keepdims=True)
+    value = collect(2)
+    retained = decay * held + match * value
     mean = jnp.mean(retained, -1, keepdims=True)
     var = jnp.mean(jnp.square(retained - mean), -1, keepdims=True)
     normed = (retained - mean) * lax.rsqrt(var + 1e-05)
+    gate_pre = collect(3)
     silu_gate = gate_pre / (1.0 + jnp.exp(-gate_pre))
-    attended = (normed * silu_gate).astype(BF16).astype(F32)
-    own_rows = pl.ds(pl.multiple_of(me * heads, heads), heads)
-    att[own_rows, :] = attended
-
-    def send_all(phase, src, dst):
+    att[me] = (normed * silu_gate).astype(BF16)
+
+    def remote(phase, src, dst, slot, chip, core):
+        return pltpu.make_async_remote_copy(
+            src_ref=src,
+            dst_ref=dst,
+            send_sem=send_sem.at[phase, slot],
+            recv_sem=recv_sem.at[phase, me],
+            device_id=(dp, chip, core),
+            device_id_type=MESH,
+        )
+
+    def send_all(phase, ref):
         copies = []
-        for d, e in steps:
-            other_kv, other_tp = partner(d, e)
-            copy = pltpu.make_async_remote_copy(
-                src_ref=src,
-                dst_ref=dst,
-                send_sem=send_sem.at[phase, d * tp_count + e],
-                recv_sem=recv_sem.at[phase, d * tp_count + e],
-                device_id=(dp, other_kv, other_tp),
-                device_id_type=MESH,
-            )
+        for chip, core in far_peers + [(kv, core) for core in beside]:
+            copy = remote(phase, ref.at[me], ref.at[me], len(copies), chip, core)
             copy.start()
             copies.append(copy)
         return copies
 
-    att_copies = send_all(0, att.at[own_rows, :], att.at[own_rows, :])
+    def wait_from(phase, ref, chip, core):
+        source = chip * tp_count + core
+        pltpu.make_async_remote_copy(
+            src_ref=ref.at[me],
+            dst_ref=ref.at[source],
+            send_sem=send_sem.at[phase, 0],
+            recv_sem=recv_sem.at[phase, source],
+            device_id=(dp, chip, core),
+            device_id_type=MESH,
+        ).wait_recv()
+
+    att_copies = send_all(0, att)
+
+    key_t = jnp.transpose(key)
+    for h in range(heads):
+        nst[h] = decay[h : h + 1, :] * state[h] + key_t[:, h : h + 1] * value[h : h + 1, :]
 
     wout_load.wait()
-    for copy in att_copies:
-        copy.wait_recv()
+    for chip, core in near_peers:
+        wait_from(0, att, chip, core)
+    for p in range(group):
+        att_rows[p * heads : (p + 1) * heads, :] = att[p].astype(F32)
     lhs = jnp.concatenate(
         [
-            att[pl.ds(t * heads + h, rows, stride=tp_count * heads), :]
+            att_rows[pl.ds(t * heads + h, rows, stride=tp_count * heads), :]
             for t in range(tp_count)
             for h in range(heads)
         ],
@@ -218,92 +283,114 @@
     ).astype(BF16)
     mixed = jnp.dot(lhs, wout[...], preferred_element_type=F32)
     tok_own = tok[:, pl.ds(pl.multiple_of(tp * cols, cols), cols)]
-    mix[me] = (tok_own.astype(F32) + mixed).astype(BF16)
-    mix_copies = send_all(1, mix.at[me], mix.at[me])
-    gmix_load.wait()
+    own = (tok_own.astype(F32) + mixed).astype(BF16)
+    mix[me] = own
+    mix_copies = send_all(1, mix)
+
+    own = own.astype(F32)
+    shift = jnp.mean(own, 1, keepdims=True)
     gout_load.wait()
-    for copy in mix_copies:
-        copy.wait_recv()
-    whole = [mix[p].astype(F32) for p in range(group)]
-    total = functools.reduce(lambda a, b: a + b, whole)
-    squares = functools.reduce(lambda a, b: a + b, [x * x for x in whole])
+    wfg_load.wait()
+    wfu_load.wait()
+    tile = 256
+    starts = list(range(0, ff, tile))
+    own_lanes = pl.ds(pl.multiple_of(me * cols, cols), cols)
+
+    def centred(x, lanes):
+        z = jnp.concatenate([x * gmix[:, lanes], jnp.zeros((8 - rows, x.shape[1]), F32)], 0)
+        return (z + gain_rows[:, lanes]).astype(BF16)
+
+    def up_part(lhs, lanes, first):
+        for start in starts:
+            at = pl.ds(start, min(tile, ff - start))
+            for weight, acc in ((wfg, acc_gate), (wfu, acc_up)):
+                part = dot_rows(lhs, weight[at, lanes])
+                acc[:, at] = part if first else acc[:, at] + part
+
+    own = own - shift
+    up_part(centred(own, own_lanes), own_lanes, True)
+    total = own
+    squares = own * own
+    for core in beside:
+        wait_from(1, mix, kv, core)
+        lanes = pl.ds(pl.multiple_of((kv * tp_count + core) * cols, cols), cols)
+        x = mix[kv * tp_count + core].astype(F32) - shift
+        total = total + x
+        squares = squares + x * x
+        up_part(centred(x, lanes), lanes, False)
+    for chip in near:
+        for core in range(tp_count):
+            wait_from(1, mix, chip, core)
+        pieces = []
+        for core in range(tp_count):
+            lanes = pl.ds(pl.multiple_of((chip * tp_count + core) * cols, cols), cols)
+            x = mix[chip * tp_count + core].astype(F32) - shift
+            total = total + x
+            squares = squares + x * x
+            pieces.append(centred(x, lanes))
+        lanes = pl.ds(pl.multiple_of(chip * (tp_count * cols), tp_count * cols), tp_count * cols)
+        up_part(jnp.concatenate(pieces, 1), lanes, False)
+
     mean = jnp.sum(total, 1, keepdims=True) / width
     var = jnp.sum(squares, 1, keepdims=True) / width - mean * mean
     scale = lax.rsqrt(var + 1e-05)
-    for p in range(group):
-        block = slice(p * cols, (p + 1) * cols)
-        hidden = ((whole[p] - mean) * scale * gmix[:, block]).astype(BF16)
-        hid[:, block] = hidden
-        hid_own[p] = hidden.astype(F32)
-
-    wfg_load.wait()
-    wfu_load.wait()
-    tile = 256
-    whole_tiles = ff // tile
-
-    def inner_block(at):
-        gate = dot_rows(hid[...], wfg[at, :])
-        upward = dot_rows(hid[...], wfu[at, :])
-        inner[:, at] = (gate / (1.0 + jnp.exp(-gate)) * upward).astype(BF16)
-
-    for j in range(whole_tiles):
-        inner_block(pl.ds(j * tile, tile))
-
-    if ff % tile:
-        inner_block(pl.ds(whole_tiles * tile, ff % tile))
+    hid_own = ((own - mean) * scale * gmix[:, own_lanes]).astype(BF16).astype(F32)
+
+    def finish(acc, at):
+        bias = acc[rows : rows + 1, at] + acc[rows + 1 : rows + 2, at]
+        return scale * (acc[:rows, at] - mean * bias)
+
+    for start in starts:
+        at = pl.ds(start, min(tile, ff - start))
+        gate = finish(acc_gate, at)
+        inner[:, at] = (gate / (1.0 + jnp.exp(-gate)) * finish(acc_up, at)).astype(BF16)
 
     wfd_load.wait()
     main = ff // 128 * 128
 
-    def down_block(owner):
-        at = pl.ds(pl.multiple_of(owner * cols, cols), cols)
+    def down_part(at):
         result = jnp.dot(inner[:, :main], wfd[:main, at], preferred_element_type=F32)
         if main < ff:
             result += jnp.dot(inner[:, main:], wfd[main:, at], preferred_element_type=F32)
         return result
 
     f_copies = []
-    for d, e in steps:
-        other_kv, other_tp = partner(d, e)
-        owner = other_kv * tp_count + other_tp
-        fsend[owner] = down_block(owner).astype(BF16)
-        copy = pltpu.make_async_remote_copy(
-            src_ref=fsend.at[owner],
-            dst_ref=frecv.at[me],
-            send_sem=send_sem.at[2, d * tp_count + e],
-            recv_sem=recv_sem.at[2, d * tp_count + e],
-            device_id=(dp, other_kv, other_tp),
-            device_id_type=MESH,
-        )
+
+    def send_down(chip, core, result):
+        owner = chip * tp_count + core
+        fsend[owner] = result.astype(BF16)
+        copy = remote(2, fsend.at[owner], frecv.at[me], len(f_copies), chip, core)
         copy.start()
-        f_copies.append((d, e, copy))
-    summed = hid_own[me] + down_block(me)
-    for d, e, copy in f_copies:
-        copy.wait_recv()
-        source = lax.rem(kv + kv_count - d, kv_count) * tp_count + lax.rem(
-            tp + tp_count - e, tp_count
-        )
-        summed = summed + frecv[source].astype(F32)
+        f_copies.append(copy)
+
+    for chip in reversed(near):
+        span = tp_count * cols
+        both = down_part(pl.ds(pl.multiple_of(chip * span, span), span))
+        for core in range(tp_count):
+            send_down(chip, core, both[:, core * cols : (core + 1) * cols])
+    for core in beside:
+        lanes = pl.ds(pl.multiple_of((kv * tp_count + core) * cols, cols), cols)
+        send_down(kv, core, down_part(lanes))
+    summed = hid_own + down_part(own_lanes)
+    for chip, core in near_peers:
+        wait_from(2, frecv, chip, core)
+        summed = summed + frecv[chip * tp_count + core].astype(F32)
     own_sum = jnp.sum(summed, 1, keepdims=True)
     own_square = jnp.sum(summed * summed, 1, keepdims=True)
     low_half = lax.broadcasted_iota(jnp.int32, (rows, 128), 1) < 64
     sums[me] = jnp.where(low_half, own_sum, own_square)
-    sum_copies = send_all(3, sums.at[me], sums.at[me])
-    for copy in sum_copies:
-        copy.wait_recv()
+    sum_copies = send_all(3, sums)
+    for chip, core in near_peers:
+        wait_from(3, sums, chip, core)
     all_sums = functools.reduce(lambda a, b: a + b, [sums[p] for p in range(group)])
     mean = all_sums[:, :1] / width
     var = all_sums[:, 64:65] / width - mean * mean
-    gain = gout[:, pl.ds(pl.multiple_of(me * cols, cols), cols)]
+    gain = gout[:, own_lanes]
     out_v[...] = ((summed - mean) * lax.rsqrt(var + 1e-05) * gain).astype(BF16)
 
-    for _, _, copy in q_copies:
-        copy.wait_send()
-    for copies in (att_copies, mix_copies, sum_copies):
+    for copies in (q_copies, att_copies, mix_copies, f_copies, sum_copies):
         for copy in copies:
             copy.wait_send()
-    for _, _, copy in f_copies:
-        copy.wait_send()
 
 
 def store_kernel(out_v, nst_v, out_h, nst_h, sem):
@@ -373,19 +460,16 @@
         + [
             pltpu.VMEM((kv_count, 4, heads, width_head), F32),
             pltpu.VMEM((kv_count, 4, heads, width_head), F32),
+            pltpu.VMEM((group, heads, width_head), BF16),
             pltpu.VMEM((group * heads, width_head), F32),
             pltpu.VMEM((group, rows, cols), BF16),
-            pltpu.VMEM((group, rows, cols), F32),
-            pltpu.VMEM((rows, width), BF16),
+            pltpu.VMEM((8, width), F32),
+            pltpu.VMEM((8, w_ffn_gate.shape[1]), F32),
+            pltpu.VMEM((8, w_ffn_gate.shape[1]), F32),
             pltpu.VMEM((rows, w_ffn_gate.shape[1]), BF16),
             pltpu.VMEM((group, rows, cols), BF16),
             pltpu.VMEM((group, rows, cols), BF16),
             pltpu.VMEM((group, rows, 128), F32),
-            pltpu.SemaphoreType.DMA((len(arrays) + 1,)),
-            pltpu.SemaphoreType.DMA((4, kv_count)),
-            pltpu.SemaphoreType.DMA((4, kv_count)),
-            pltpu.SemaphoreType.DMA((4, group)),
-            pltpu.SemaphoreType.DMA((4, group)),
         ],
         compiler_params=pltpu.CompilerParams(
             collective_id=0, has_side_effects=True, vmem_limit_bytes=56 * 2**20
@@ -412,6 +496,7 @@
         and width_head == 128
         and w_out.shape[1] % 128 == 0
         and tokens.shape[0] == kv_count
+        and kv_count <= 6
         and kv_count * tp_count <= 16
     )
 

time: 37.3 us -> 31.3 us (0.84)
  Pallas kernels: 35.8 us -> 29.8 us
    pallas_call x1, Pallas kernels: 35 us -> 29 us  [fused_step(): pl.pallas_call(functools.partial(step_kernel, kv_count, tp_count), out_sh...]
where the time goes in v1:
time: 31.3 us; the launch traced here: 31.1 us
  Pallas kernels  29.8 us (95%)
  between operations  1.29 us (4%)
    pallas_call x1, Pallas kernels, fused_step(): pl.pallas_call(functools.partial(step_kernel, kv_count, tp_count), out_sh...  29 us
    pallas_call x1, Pallas kernels, fused_step(): pl.pallas_call(store_kernel, out_shape=(jax.ShapeDtypeStruct(out.shape, o...  0.81 us

profile of v1, /device:TPU:0, one launch (start us, length us, event | category | flops | bytes accessed | tf_op | source)
XLA Modules:
  0.0 31.1 jit_solution(1512839231559921809)
XLA Ops:
  1.3 29.0 %shard_map.149 = (bf16[4,512]{1,0:T(4,128)(2,1)S(1)}, f32[8,128,128]{2,1,0:T(8,128)S(1)}) custom-call(bf16[4,1024]{1,0:T(4,128)(2,1)} %refs_0_.1, s32[1,1]{1,0:T(1,128)} %bitcast.7.refs_1_, f32[8,128,128]{2,1,0:T(8,128)} %bitcast.10, bf16[1024,1024]{1,0:T(8,128)(2,1)} %refs_3_.1, bf16[1024,1024]{1,0:T(8,128)(2,1)} %refs_4_.1, bf16[1024,1024]{1,0:T(8,128)(2,1)} %refs_5_.1, ...), custom_call_target="tpu_custom_call" | custom-call | tf_op jit(solution)/shard_map/pallas_call | solution.py:451
  30.3 0.8 %shard_map.150 = (bf16[4,512]{1,0:T(4,128)(2,1)}, f32[8,128,128]{2,1,0:T(8,128)}) custom-call(bf16[4,512]{1,0:T(4,128)(2,1)S(1)} %get-tuple-element.6.out_v, f32[8,128,128]{2,1,0:T(8,128)S(1)} %get-tuple-element.7.nst_v), custom_call_target="tpu_custom_call" | custom-call | tf_op jit(solution)/shard_map/pallas_call | solution.py:478

commit v2 on v1

--- a/solution.py
+++ b/solution.py
@@ -17,30 +17,22 @@
     return lax.dot_general(values, weight, (((1,), (1,)), ((), ())), preferred_element_type=F32)
 
 
-def near_first(kv, count):
+def nearest(kv, count, k):
     low = jnp.minimum(kv, count - 1 - kv)
     step = jnp.where(2 * kv < count, 1, -1)
-    order = []
-    for k in range(1, count):
-        offset = jnp.where(
-            k <= 2 * low, (k + 1) // 2 * (1 if k % 2 == 0 else -1), (k - low) * step
-        )
-        order.append(kv + offset)
-    return order
+    side = 1 - 2 * (k % 2)
+    return kv + jnp.where(k <= 2 * low, (k + 1) // 2 * side, (k - low) * step)
 
 
 def step_kernel(kv_count, tp_count, *refs):
-    operands = 14
-
-    def body(local_sem, q_send_sem, q_recv_sem, send_sem, recv_sem):
-        step_body(
-            kv_count, tp_count, *refs, local_sem, q_send_sem, q_recv_sem, send_sem, recv_sem
-        )
+    def body(*sems):
+        step_body(kv_count, tp_count, *refs, *sems)
 
     group = kv_count * tp_count
     pl.run_scoped(
         body,
-        pltpu.SemaphoreType.DMA((operands,)),
+        pltpu.SemaphoreType.DMA((13,)),
+        pltpu.SemaphoreType.DMA((kv_count, 2)),
         pltpu.SemaphoreType.DMA((4, kv_count)),
         pltpu.SemaphoreType.DMA((4, kv_count)),
         pltpu.SemaphoreType.DMA((4, group)),
@@ -76,24 +68,28 @@
     wg,
     wout,
     gmix,
-    wfg,
-    wfu,
+    w_up,
     wfd,
     gout,
     inv,
     qsend,
     qrecv,
+    half_part,
+    mixed_part,
     att,
     att_rows,
     mix,
     gain_rows,
     acc_gate,
     acc_up,
+    turned,
+    eye,
     inner,
     fsend,
     frecv,
     sums,
     local_sem,
+    up_sem,
     q_send_sem,
     q_recv_sem,
     send_sem,
@@ -107,19 +103,15 @@
     rows = tok.shape[0]
     heads = state.shape[0]
     width_head = state.shape[1]
-    width = wfg.shape[1]
+    width = w_up.shape[2]
     cols = mix.shape[2]
-    ff = wfg.shape[0]
-
-    near = near_first(kv, kv_count)
+    ff = w_up.shape[1]
+
+    near = [nearest(kv, kv_count, k) for k in range(1, kv_count)]
     beside = [lax.rem(tp + e, tp_count) for e in range(1, tp_count)]
     far_peers = [(chip, core) for chip in reversed(near) for core in range(tp_count)]
     near_peers = [(kv, core) for core in beside]
     near_peers += [(chip, core) for chip in near for core in range(tp_count)]
-
-    barrier = pltpu.get_barrier_semaphore()
-    for chip, core in far_peers + [(kv, core) for core in beside]:
-        pl.semaphore_signal(barrier, inc=1, device_id=(dp, chip, core), device_id_type=MESH)
 
     loads = []
 
@@ -132,16 +124,27 @@
     tok_load = load(tok_h, tok)
     pos_load = load(pos_h, pos)
     inv_load = load(inv_h, inv)
-    proj_loads = [
-        load(src, dst) for src, dst in ((wq_h, wq), (wk_h, wk), (wv_h, wv), (wg_h, wg))
-    ]
+    deep = wg.shape[0] // 2
+    halves = [pl.ds(0, deep), pl.ds(deep, deep)]
+    proj_loads = [[load(src, dst)] for src, dst in ((wq_h, wq), (wk_h, wk), (wv_h, wv))]
+    proj_loads.append([load(wg_h.at[half], wg.at[half]) for half in halves])
     state_load = load(state_h, state)
     gmix_load = load(gmix_h, gmix)
     gout_load = load(gout_h, gout)
 
+    barrier = pltpu.get_barrier_semaphore()
+    for chip, core in far_peers + [(kv, core) for core in beside]:
+        pl.semaphore_signal(barrier, inc=1, device_id=(dp, chip, core), device_id_type=MESH)
+
     pos_load.wait()
     inv_load.wait()
     lane = lax.broadcasted_iota(jnp.int32, (1, width_head), 1)
+    eye[...] = jnp.where(
+        lax.broadcasted_iota(jnp.int32, eye.shape, 0)
+        == lax.broadcasted_iota(jnp.int32, eye.shape, 1),
+        1.0,
+        0.0,
+    ).astype(BF16)
     angle = pos[...].astype(F32) * inv[...]
     cosine = jnp.cos(angle)
     sine = jnp.sin(angle)
@@ -149,12 +152,10 @@
 
     tok_load.wait()
     later = []
-    q_copies = []
-
-    def send_part(p):
-        for d in range(kv_count - 1, 0, -1):
-            chip = near[d - 1]
-            copy = pltpu.make_async_remote_copy(
+
+    def part_copies(p):
+        return [
+            pltpu.make_async_remote_copy(
                 src_ref=qsend.at[chip, p],
                 dst_ref=qrecv.at[kv, p],
                 send_sem=q_send_sem.at[p, d],
@@ -162,26 +163,61 @@
                 device_id=(dp, chip, tp),
                 device_id_type=MESH,
             )
-            copy.start()
-            q_copies.append(copy)
-
-    following = ((wout_h, wout), (wfg_h, wfg), (wfu_h, wfu), (wfd_h, wfd))
+            for d, chip in reversed(list(enumerate(near)))
+        ]
+
+    span = tp_count * cols
+
+    def chip_lanes(chip):
+        return pl.ds(pl.multiple_of(chip * span, span), span)
+
+    def up_copy(rank, m):
+        chip = nearest(kv, kv_count, kv_count - 1 - rank)
+        at = chip_lanes(chip)
+        source = (wfg_h, wfu_h)[m] if isinstance(m, int) else wfg_h
+        return pltpu.make_async_copy(source.at[:, at], w_up.at[m, :, at], up_sem.at[rank, m])
+
+    stage = jnp.minimum(kv_count - 1 - kv, 3)
     for p, weight in enumerate((wq, wk, wv, wg)):
-        proj_loads[p].wait()
-        later.append(load(*following[p]))
-        part = jnp.dot(tok[...], weight[...], preferred_element_type=F32)
+        proj_loads[p][0].wait()
+        if p == 0:
+            later.append(load(wout_h, wout))
+        ranks = [p] if p < 3 else list(range(3, kv_count))
+        for rank in ranks:
+            for m in range(2):
+                up_copy(rank, m).start()
+        if p < 3:
+            part = jnp.dot(tok[...], weight[...], preferred_element_type=F32)
+        else:
+            later.append(load(wfd_h, wfd))
+            half_part[...] = jnp.dot(
+                tok[:, :deep], weight[:deep], preferred_element_type=F32
+            )
+            proj_loads[p][1].wait()
+            part = half_part[...] + jnp.dot(
+                tok[:, deep:], weight[deep:], preferred_element_type=F32
+            )
         for i in range(kv_count):
             for h in range(heads):
                 qsend[i, p, h : h + 1, :] = part[
                     i : i + 1, h * width_head : (h + 1) * width_head
                 ]
-        if p == 2:
+
+        @pl.when(stage == p)
+        def first_sends():
             pl.semaphore_wait(barrier, group - 1)
-            for done in range(3):
-                send_part(done)
-        elif p == 3:
-            send_part(p)
-    wout_load, wfg_load, wfu_load, wfd_load = later
+            for done in range(p + 1):
+                for copy in part_copies(done):
+                    copy.start()
+
+        if p > 0:
+
+            @pl.when(stage < p)
+            def next_send():
+                for copy in part_copies(p):
+                    copy.start()
+
+    wout_load, wfd_load = later
 
     head_id = (tp * heads + lax.broadcasted_iota(jnp.int32, (heads, width_head), 0)).astype(F32)
     total_heads = heads * tp_count
@@ -212,6 +248,31 @@
             total = total + qrecv[chip, p]
         return total
 
+    pieces = 2 * (kv_count - 1)
+    turned_early = functools.reduce(
+        lambda a, b: a + b,
+        [jnp.where(kv == c, max(pieces // (c + 1) - 1 + min(c, 1), 0), 0) for c in range(kv_count - 1)],
+    )
+
+    def turn(piece, carry):
+        rank = piece // 2
+        m = piece % 2
+        up_copy(rank, m).wait()
+        start = nearest(kv, kv_count, kv_count - 1 - rank) * span
+        for k in range(0, span, 512):
+            for f in range(0, ff, 256):
+                n = min(256, ff - f)
+                at = pl.ds(pl.multiple_of(start + k, 256), 256)
+                turned[piece, k : k + 256, f : f + n] = dot_rows(
+                    eye[...], w_up[m, f : f + n, at]
+                ).astype(BF16)
+                if k + 256 < span:
+                    at = pl.ds(pl.multiple_of(start + k + 256, 256), 256)
+                    turned[piece, k + 256 : k + 512, f : f + n] = w_up[m, f : f + n, at].T
+        return carry
+
+    lax.fori_loop(0, turned_early, turn, 0)
+
     state_load.wait()
     query = rotate_row(collect(0))
     query_t = jnp.transpose(query)
@@ -268,20 +329,36 @@
     for h in range(heads):
         nst[h] = decay[h : h + 1, :] * state[h] + key_t[:, h : h + 1] * value[h : h + 1, :]
 
+    lax.fori_loop(turned_early, pieces, turn, 0)
+
     wout_load.wait()
-    for chip, core in near_peers:
-        wait_from(0, att, chip, core)
-    for p in range(group):
-        att_rows[p * heads : (p + 1) * heads, :] = att[p].astype(F32)
-    lhs = jnp.concatenate(
-        [
-            att_rows[pl.ds(t * heads + h, rows, stride=tp_count * heads), :]
-            for t in range(tp_count)
-            for h in range(heads)
-        ],
-        axis=1,
-    ).astype(BF16)
-    mixed = jnp.dot(lhs, wout[...], preferred_element_type=F32)
+    mixed = None
+    for t in reversed(range(tp_count)):
+        for chip in near:
+            wait_from(0, att, chip, t)
+
+        @pl.when(tp != t)
+        def wait_beside():
+            wait_from(0, att, kv, t)
+
+        for i in range(kv_count):
+            start = (i * tp_count + t) * heads
+            att_rows[start : start + heads, :] = att[i * tp_count + t].astype(F32)
+        lhs = jnp.concatenate(
+            [
+                att_rows[pl.ds(t * heads + h, rows, stride=tp_count * heads), :]
+                for h in range(heads)
+            ],
+            axis=1,
+        ).astype(BF16)
+        depth = heads * width_head
+        part = jnp.dot(lhs, wout[t * depth : (t + 1) * depth], preferred_element_type=F32)
+        if t > 0:
+            if t < tp_count - 1:
+                part = part + mixed_part[...]
+            mixed_part[...] = part
+        else:
+            mixed = part + mixed_part[...]
     tok_own = tok[:, pl.ds(pl.multiple_of(tp * cols, cols), cols)]
     own = (tok_own.astype(F32) + mixed).astype(BF16)
     mix[me] = own
@@ -290,8 +367,8 @@
     own = own.astype(F32)
     shift = jnp.mean(own, 1, keepdims=True)
     gout_load.wait()
-    wfg_load.wait()
-    wfu_load.wait()
+    for m in range(2):
+        up_copy(kv_count - 1, m).wait()
     tile = 256
     starts = list(range(0, ff, tile))
     own_lanes = pl.ds(pl.multiple_of(me * cols, cols), cols)
@@ -300,11 +377,19 @@
         z = jnp.concatenate([x * gmix[:, lanes], jnp.zeros((8 - rows, x.shape[1]), F32)], 0)
         return (z + gain_rows[:, lanes]).astype(BF16)
 
+    def up_turned(lhs, rank):
+        for start in starts:
+            at = pl.ds(start, min(tile, ff - start))
+            for m, acc in enumerate((acc_gate, acc_up)):
+                acc[:, at] += jnp.dot(
+                    lhs, turned[2 * rank + m, :, at], preferred_element_type=F32
+                )
+
     def up_part(lhs, lanes, first):
         for start in starts:
             at = pl.ds(start, min(tile, ff - start))
-            for weight, acc in ((wfg, acc_gate), (wfu, acc_up)):
-                part = dot_rows(lhs, weight[at, lanes])
+            for m, acc in enumerate((acc_gate, acc_up)):
+                part = dot_rows(lhs, w_up[m, at, lanes])
                 acc[:, at] = part if first else acc[:, at] + part
 
     own = own - shift
@@ -318,18 +403,19 @@
         total = total + x
         squares = squares + x * x
         up_part(centred(x, lanes), lanes, False)
-    for chip in near:
+    for k, chip in enumerate(near):
         for core in range(tp_count):
             wait_from(1, mix, chip, core)
-        pieces = []
+        if k == kv_count - 2:
+            wfd_load.wait()
+        blocks = []
         for core in range(tp_count):
             lanes = pl.ds(pl.multiple_of((chip * tp_count + core) * cols, cols), cols)
             x = mix[chip * tp_count + core].astype(F32) - shift
             total = total + x
             squares = squares + x * x
-            pieces.append(centred(x, lanes))
-        lanes = pl.ds(pl.multiple_of(chip * (tp_count * cols), tp_count * cols), tp_count * cols)
-        up_part(jnp.concatenate(pieces, 1), lanes, False)
+            blocks.append(centred(x, lanes))
+        up_turned(jnp.concatenate(blocks, 1), kv_count - 2 - k)
 
     mean = jnp.sum(total, 1, keepdims=True) / width
     var = jnp.sum(squares, 1, keepdims=True) / width - mean * mean
@@ -345,7 +431,6 @@
         gate = finish(acc_gate, at)
         inner[:, at] = (gate / (1.0 + jnp.exp(-gate)) * finish(acc_up, at)).astype(BF16)
 
-    wfd_load.wait()
     main = ff // 128 * 128
 
     def down_part(at):
@@ -364,8 +449,7 @@
         f_copies.append(copy)
 
     for chip in reversed(near):
-        span = tp_count * cols
-        both = down_part(pl.ds(pl.multiple_of(chip * span, span), span))
+        both = down_part(chip_lanes(chip))
         for core in range(tp_count):
             send_down(chip, core, both[:, core * cols : (core + 1) * cols])
     for core in beside:
@@ -388,7 +472,10 @@
     gain = gout[:, own_lanes]
     out_v[...] = ((summed - mean) * lax.rsqrt(var + 1e-05) * gain).astype(BF16)
 
-    for copies in (q_copies, att_copies, mix_copies, f_copies, sum_copies):
+    for p in range(4):
+        for copy in part_copies(p):
+            copy.wait_send()
+    for copies in (att_copies, mix_copies, f_copies, sum_copies):
         for copy in copies:
             copy.wait_send()
 
@@ -446,6 +533,7 @@
         jnp.asarray(inverse),
     )
     held = [pltpu.VMEM(a.shape, a.dtype) for a in arrays]
+    held[9:11] = [pltpu.VMEM((2, w_ffn_gate.shape[1], width), BF16)]
     vmem_spec = pl.BlockSpec(memory_space=pltpu.VMEM)
     any_spec = pl.BlockSpec(memory_space=pl.ANY)
     out, new_state = pl.pallas_call(
@@ -460,19 +548,23 @@
         + [
             pltpu.VMEM((kv_count, 4, heads, width_head), F32),
             pltpu.VMEM((kv_count, 4, heads, width_head), F32),
+            pltpu.VMEM((rows, heads * width_head), F32),
+            pltpu.VMEM((rows, cols), F32),
             pltpu.VMEM((group, heads, width_head), BF16),
             pltpu.VMEM((group * heads, width_head), F32),
             pltpu.VMEM((group, rows, cols), BF16),
             pltpu.VMEM((8, width), F32),
             pltpu.VMEM((8, w_ffn_gate.shape[1]), F32),
             pltpu.VMEM((8, w_ffn_gate.shape[1]), F32),
+            pltpu.VMEM((2 * (kv_count - 1), tp_count * cols, w_ffn_gate.shape[1]), BF16),
+            pltpu.VMEM((256, 256), BF16),
             pltpu.VMEM((rows, w_ffn_gate.shape[1]), BF16),
             pltpu.VMEM((group, rows, cols), BF16),
             pltpu.VMEM((group, rows, cols), BF16),
             pltpu.VMEM((group, rows, 128), F32),
         ],
         compiler_params=pltpu.CompilerParams(
-            collective_id=0, has_side_effects=True, vmem_limit_bytes=56 * 2**20
+            collective_id=0, has_side_effects=True, vmem_limit_bytes=63 * 2**20
         ),
     )(*arrays)
     out, new_state = pl.pallas_call(
@@ -494,9 +586,10 @@
     return (
         seqs == 1
         and width_head == 128
-        and w_out.shape[1] % 128 == 0
+        and w_out.shape[1] % 256 == 0
         and tokens.shape[0] == kv_count
-        and kv_count <= 6
+        and 3 <= kv_count <= 6
+        and tp_count >= 2
         and kv_count * tp_count <= 16
     )
 

time: 31.3 us -> 28.6 us (0.914)
  Pallas kernels: 29.8 us -> 27.1 us
    pallas_call x1, Pallas kernels: 29 us -> 26.3 us  [fused_step(): pl.pallas_call(functools.partial(step_kernel, kv_count, tp_count), out_sh...]
where the time goes in v2:
time: 28.6 us; the launch traced here: 28.4 us
  Pallas kernels  27.1 us (95%)
  between operations  1.29 us (5%)
    pallas_call x1, Pallas kernels, fused_step(): pl.pallas_call(functools.partial(step_kernel, kv_count, tp_count), out_sh...  26.3 us
    pallas_call x1, Pallas kernels, fused_step(): pl.pallas_call(store_kernel, out_shape=(jax.ShapeDtypeStruct(out.shape, o...  0.81 us

profile of v2, /device:TPU:0, one launch (start us, length us, event | category | flops | bytes accessed | tf_op | source)
XLA Modules:
  0.0 28.4 jit_solution(8818277082357514934)
XLA Ops:
  1.3 26.3 %shard_map.149 = (bf16[4,512]{1,0:T(4,128)(2,1)S(1)}, f32[8,128,128]{2,1,0:T(8,128)S(1)}) custom-call(bf16[4,1024]{1,0:T(4,128)(2,1)} %refs_0_.1, s32[1,1]{1,0:T(1,128)} %bitcast.7.refs_1_, f32[8,128,128]{2,1,0:T(8,128)} %bitcast.10, bf16[1024,1024]{1,0:T(8,128)(2,1)} %refs_3_.1, bf16[1024,1024]{1,0:T(8,128)(2,1)} %refs_4_.1, bf16[1024,1024]{1,0:T(8,128)(2,1)} %refs_5_.1, ...), custom_call_target="tpu_custom_call" | custom-call | tf_op jit(solution)/shard_map/pallas_call | solution.py:539
  27.6 0.8 %shard_map.150 = (bf16[4,512]{1,0:T(4,128)(2,1)}, f32[8,128,128]{2,1,0:T(8,128)}) custom-call(bf16[4,512]{1,0:T(4,128)(2,1)S(1)} %get-tuple-element.6.out_v, f32[8,128,128]{2,1,0:T(8,128)S(1)} %get-tuple-element.7.nst_v), custom_call_target="tpu_custom_call" | custom-call | tf_op jit(solution)/shard_map/pallas_call | solution.py:570

commit v3 on v2

--- a/solution.py
+++ b/solution.py
@@ -35,6 +35,7 @@
         pltpu.SemaphoreType.DMA((kv_count, 2)),
         pltpu.SemaphoreType.DMA((4, kv_count)),
         pltpu.SemaphoreType.DMA((4, kv_count)),
+        pltpu.SemaphoreType.DMA((2, tp_count)),
         pltpu.SemaphoreType.DMA((4, group)),
         pltpu.SemaphoreType.DMA((4, group)),
     )
@@ -76,8 +77,9 @@
     qrecv,
     half_part,
     mixed_part,
+    gate_recv,
+    gates,
     att,
-    att_rows,
     mix,
     gain_rows,
     acc_gate,
@@ -92,6 +94,7 @@
     up_sem,
     q_send_sem,
     q_recv_sem,
+    gate_sem,
     send_sem,
     recv_sem,
 ):
@@ -156,8 +159,8 @@
     def part_copies(p):
         return [
             pltpu.make_async_remote_copy(
-                src_ref=qsend.at[chip, p],
-                dst_ref=qrecv.at[kv, p],
+                src_ref=qsend.at[chip, p] if p < 3 else half_part,
+                dst_ref=qrecv.at[kv, p] if p < 3 else gate_recv.at[kv],
                 send_sem=q_send_sem.at[p, d],
                 recv_sem=q_recv_sem.at[p, kv],
                 device_id=(dp, chip, tp),
@@ -194,10 +197,10 @@
                 tok[:, :deep], weight[:deep], preferred_element_type=F32
             )
             proj_loads[p][1].wait()
-            part = half_part[...] + jnp.dot(
+            half_part[...] += jnp.dot(
                 tok[:, deep:], weight[deep:], preferred_element_type=F32
             )
-        for i in range(kv_count):
+        for i in range(kv_count if p < 3 else 0):
             for h in range(heads):
                 qsend[i, p, h : h + 1, :] = part[
                     i : i + 1, h * width_head : (h + 1) * width_head
@@ -206,11 +209,11 @@
         @pl.when(stage == p)
         def first_sends():
             pl.semaphore_wait(barrier, group - 1)
-            for done in range(p + 1):
+            for done in range(min(p, 2) + 1):
                 for copy in part_copies(done):
                     copy.start()
 
-        if p > 0:
+        if 0 < p < 3:
 
             @pl.when(stage < p)
             def next_send():
@@ -235,24 +238,30 @@
         return x * cosine + pltpu.roll(x, width_head // 2, 1) * sine
 
     def collect(p):
-        total = qsend[kv, p]
+        total = qsend[kv, p] if p < 3 else half_part[...]
         for chip in near:
+            landed = qrecv.at[chip, p] if p < 3 else gate_recv.at[chip]
             pltpu.make_async_remote_copy(
-                src_ref=qsend.at[chip, p],
-                dst_ref=qrecv.at[chip, p],
+                src_ref=landed,
+                dst_ref=landed,
                 send_sem=q_send_sem.at[p, 0],
                 recv_sem=q_recv_sem.at[p, chip],
                 device_id=(dp, chip, tp),
                 device_id_type=MESH,
             ).wait_recv()
-            total = total + qrecv[chip, p]
+            total = total + landed[...]
         return total
 
     pieces = 2 * (kv_count - 1)
-    turned_early = functools.reduce(
-        lambda a, b: a + b,
-        [jnp.where(kv == c, max(pieces // (c + 1) - 1 + min(c, 1), 0), 0) for c in range(kv_count - 1)],
-    )
+
+    def by_kv(values):
+        return functools.reduce(
+            lambda a, b: a + b, [jnp.where(kv == c, n, 0) for c, n in enumerate(values)]
+        )
+
+    middle = [pieces // 3] * (kv_count - 2)
+    turns = [by_kv([2]), by_kv([pieces - 1] + middle + [1])]
+    turns.append(by_kv([pieces] + [n + 2 for n in middle] + [3]))
 
     def turn(piece, carry):
         rank = piece // 2
@@ -271,7 +280,10 @@
                     turned[piece, k + 256 : k + 512, f : f + n] = w_up[m, f : f + n, at].T
         return carry
 
-    lax.fori_loop(0, turned_early, turn, 0)
+    lax.fori_loop(0, turns[0], turn, 0)
+    for copy in part_copies(3):
+        copy.start()
+    lax.fori_loop(turns[0], turns[1], turn, 0)
 
     state_load.wait()
     query = rotate_row(collect(0))
@@ -290,9 +302,7 @@
     mean = jnp.mean(retained, -1, keepdims=True)
     var = jnp.mean(jnp.square(retained - mean), -1, keepdims=True)
     normed = (retained - mean) * lax.rsqrt(var + 1e-05)
-    gate_pre = collect(3)
-    silu_gate = gate_pre / (1.0 + jnp.exp(-gate_pre))
-    att[me] = (normed * silu_gate).astype(BF16)
+    att[me] = normed
 
     def remote(phase, src, dst, slot, chip, core):
         return pltpu.make_async_remote_copy(
@@ -325,11 +335,29 @@
 
     att_copies = send_all(0, att)
 
+    lax.fori_loop(turns[1], turns[2], turn, 0)
+
+    gate_pre = collect(3)
+    gates[tp] = gate_pre / (1.0 + jnp.exp(-gate_pre))
+
+    def gate_copy(core):
+        return pltpu.make_async_remote_copy(
+            src_ref=gates.at[tp],
+            dst_ref=gates.at[tp],
+            send_sem=gate_sem.at[0, core],
+            recv_sem=gate_sem.at[1, tp],
+            device_id=(dp, kv, core),
+            device_id_type=MESH,
+        )
+
+    for core in beside:
+        gate_copy(core).start()
+
     key_t = jnp.transpose(key)
     for h in range(heads):
         nst[h] = decay[h : h + 1, :] * state[h] + key_t[:, h : h + 1] * value[h : h + 1, :]
 
-    lax.fori_loop(turned_early, pieces, turn, 0)
+    lax.fori_loop(turns[2], pieces, turn, 0)
 
     wout_load.wait()
     mixed = None
@@ -340,17 +368,19 @@
         @pl.when(tp != t)
         def wait_beside():
             wait_from(0, att, kv, t)
-
-        for i in range(kv_count):
-            start = (i * tp_count + t) * heads
-            att_rows[start : start + heads, :] = att[i * tp_count + t].astype(F32)
+            pltpu.make_async_remote_copy(
+                src_ref=gates.at[t],
+                dst_ref=gates.at[t],
+                send_sem=gate_sem.at[0, t],
+                recv_sem=gate_sem.at[1, t],
+                device_id=(dp, kv, t),
+                device_id_type=MESH,
+            ).wait_recv()
+
         lhs = jnp.concatenate(
-            [
-                att_rows[pl.ds(t * heads + h, rows, stride=tp_count * heads), :]
-                for h in range(heads)
-            ],
-            axis=1,
-        ).astype(BF16)
+            [att[pl.ds(t, rows, stride=tp_count), h, :] for h in range(heads)], axis=1
+        )
+        lhs = (lhs * gates[t]).astype(BF16)
         depth = heads * width_head
         part = jnp.dot(lhs, wout[t * depth : (t + 1) * depth], preferred_element_type=F32)
         if t > 0:
@@ -461,23 +491,28 @@
         summed = summed + frecv[chip * tp_count + core].astype(F32)
     own_sum = jnp.sum(summed, 1, keepdims=True)
     own_square = jnp.sum(summed * summed, 1, keepdims=True)
-    low_half = lax.broadcasted_iota(jnp.int32, (rows, 128), 1) < 64
-    sums[me] = jnp.where(low_half, own_sum, own_square)
+    own_sums = [jnp.broadcast_to(x, (rows, 128)) for x in (own_sum, own_square)]
+    sums[me] = jnp.concatenate(own_sums, 1)
     sum_copies = send_all(3, sums)
+    for p in range(4):
+        for copy in part_copies(p):
+            copy.wait_send()
+    for core in beside:
+        gate_copy(core).wait_send()
+    for copies in (att_copies, mix_copies, f_copies):
+        for copy in copies:
+            copy.wait_send()
     for chip, core in near_peers:
         wait_from(3, sums, chip, core)
     all_sums = functools.reduce(lambda a, b: a + b, [sums[p] for p in range(group)])
-    mean = all_sums[:, :1] / width
-    var = all_sums[:, 64:65] / width - mean * mean
-    gain = gout[:, own_lanes]
-    out_v[...] = ((summed - mean) * lax.rsqrt(var + 1e-05) * gain).astype(BF16)
-
-    for p in range(4):
-        for copy in part_copies(p):
-            copy.wait_send()
-    for copies in (att_copies, mix_copies, f_copies, sum_copies):
-        for copy in copies:
-            copy.wait_send()
+    mean = all_sums[:, :128] / width
+    var = all_sums[:, 128:] / width - mean * mean
+    scale = lax.rsqrt(var + 1e-05)
+    mean, scale = [jnp.concatenate([x] * (cols // 128), 1) for x in (mean, scale)]
+    out_v[...] = ((summed - mean) * scale * gout[:, own_lanes]).astype(BF16)
+
+    for copy in sum_copies:
+        copy.wait_send()
 
 
 def store_kernel(out_v, nst_v, out_h, nst_h, sem):
@@ -546,12 +581,13 @@
         out_specs=(vmem_spec, vmem_spec),
         scratch_shapes=held
         + [
-            pltpu.VMEM((kv_count, 4, heads, width_head), F32),
-            pltpu.VMEM((kv_count, 4, heads, width_head), F32),
+            pltpu.VMEM((kv_count, 3, heads, width_head), F32),
+            pltpu.VMEM((kv_count, 3, heads, width_head), F32),
             pltpu.VMEM((rows, heads * width_head), F32),
             pltpu.VMEM((rows, cols), F32),
-            pltpu.VMEM((group, heads, width_head), BF16),
-            pltpu.VMEM((group * heads, width_head), F32),
+            pltpu.VMEM((kv_count, rows, heads * width_head), F32),
+            pltpu.VMEM((tp_count, rows, heads * width_head), F32),
+            pltpu.VMEM((group, heads, width_head), F32),
             pltpu.VMEM((group, rows, cols), BF16),
             pltpu.VMEM((8, width), F32),
             pltpu.VMEM((8, w_ffn_gate.shape[1]), F32),
@@ -561,7 +597,7 @@
             pltpu.VMEM((rows, w_ffn_gate.shape[1]), BF16),
             pltpu.VMEM((group, rows, cols), BF16),
             pltpu.VMEM((group, rows, cols), BF16),
-            pltpu.VMEM((group, rows, 128), F32),
+            pltpu.VMEM((group, rows, 256), F32),
         ],
         compiler_params=pltpu.CompilerParams(
             collective_id=0, has_side_effects=True, vmem_limit_bytes=63 * 2**20

time: 28.6 us -> 28.3 us (0.990)
  Pallas kernels: 27.1 us -> 26.8 us
    pallas_call x1, Pallas kernels: 26.3 us -> 26 us  [fused_step(): pl.pallas_call(functools.partial(step_kernel, kv_count, tp_count), out_sh...]
where the time goes in v3:
time: 28.3 us; the launch traced here: 28.1 us
  Pallas kernels  26.8 us (95%)
  between operations  1.29 us (5%)
    pallas_call x1, Pallas kernels, fused_step(): pl.pallas_call(functools.partial(step_kernel, kv_count, tp_count), out_sh...  26 us
    pallas_call x1, Pallas kernels, fused_step(): pl.pallas_call(store_kernel, out_shape=(jax.ShapeDtypeStruct(out.shape, o...  0.81 us

profile of v3, /device:TPU:0, one launch (start us, length us, event | category | flops | bytes accessed | tf_op | source)
XLA Modules:
  0.0 28.1 jit_solution(14235593769404583861)
XLA Ops:
  1.3 26.0 %shard_map.149 = (bf16[4,512]{1,0:T(4,128)(2,1)S(1)}, f32[8,128,128]{2,1,0:T(8,128)S(1)}) custom-call(bf16[4,1024]{1,0:T(4,128)(2,1)} %refs_0_.1, s32[1,1]{1,0:T(1,128)} %bitcast.7.refs_1_, f32[8,128,128]{2,1,0:T(8,128)} %bitcast.10, bf16[1024,1024]{1,0:T(8,128)(2,1)} %refs_3_.1, bf16[1024,1024]{1,0:T(8,128)(2,1)} %refs_4_.1, bf16[1024,1024]{1,0:T(8,128)(2,1)} %refs_5_.1, ...), custom_call_target="tpu_custom_call" | custom-call | tf_op jit(solution)/shard_map/pallas_call | solution.py:574
  27.3 0.8 %shard_map.150 = (bf16[4,512]{1,0:T(4,128)(2,1)}, f32[8,128,128]{2,1,0:T(8,128)}) custom-call(bf16[4,512]{1,0:T(4,128)(2,1)S(1)} %get-tuple-element.6.out_v, f32[8,128,128]{2,1,0:T(8,128)S(1)} %get-tuple-element.7.nst_v), custom_call_target="tpu_custom_call" | custom-call | tf_op jit(solution)/shard_map/pallas_call | solution.py:606

commit v4 on v3

--- a/solution.py
+++ b/solution.py
@@ -407,12 +407,12 @@
         z = jnp.concatenate([x * gmix[:, lanes], jnp.zeros((8 - rows, x.shape[1]), F32)], 0)
         return (z + gain_rows[:, lanes]).astype(BF16)
 
-    def up_turned(lhs, rank):
+    def up_turned(lhs, rank, depth):
         for start in starts:
             at = pl.ds(start, min(tile, ff - start))
             for m, acc in enumerate((acc_gate, acc_up)):
                 acc[:, at] += jnp.dot(
-                    lhs, turned[2 * rank + m, :, at], preferred_element_type=F32
+                    lhs, turned[2 * rank + m, depth, at], preferred_element_type=F32
                 )
 
     def up_part(lhs, lanes, first):
@@ -434,18 +434,21 @@
         squares = squares + x * x
         up_part(centred(x, lanes), lanes, False)
     for k, chip in enumerate(near):
-        for core in range(tp_count):
-            wait_from(1, mix, chip, core)
+        order = list(reversed(range(tp_count)))
         if k == kv_count - 2:
             wfd_load.wait()
-        blocks = []
-        for core in range(tp_count):
-            lanes = pl.ds(pl.multiple_of((chip * tp_count + core) * cols, cols), cols)
-            x = mix[chip * tp_count + core].astype(F32) - shift
-            total = total + x
-            squares = squares + x * x
-            blocks.append(centred(x, lanes))
-        up_turned(jnp.concatenate(blocks, 1), kv_count - 2 - k)
+        for part in [[core] for core in order] if k in (0,) else [order]:
+            for core in part:
+                wait_from(1, mix, chip, core)
+            blocks = []
+            for core in sorted(part):
+                lanes = pl.ds(pl.multiple_of((chip * tp_count + core) * cols, cols), cols)
+                x = mix[chip * tp_count + core].astype(F32) - shift
+                total = total + x
+                squares = squares + x * x
+                blocks.append(centred(x, lanes))
+            depth = pl.ds(min(part) * cols, len(part) * cols)
+            up_turned(jnp.concatenate(blocks, 1), kv_count - 2 - k, depth)
 
     mean = jnp.sum(total, 1, keepdims=True) / width
     var = jnp.sum(squares, 1, keepdims=True) / width - mean * mean

time: 28.3 us -> 28.1 us (level)
  no operation moved by 1% of the time
where the time goes in v4:
time: 28.1 us; the launch traced here: 27.9 us
  Pallas kernels  26.6 us (95%)
  between operations  1.29 us (5%)
    pallas_call x1, Pallas kernels, fused_step(): pl.pallas_call(functools.partial(step_kernel, kv_count, tp_count), out_sh...  25.8 us
    pallas_call x1, Pallas kernels, fused_step(): pl.pallas_call(store_kernel, out_shape=(jax.ShapeDtypeStruct(out.shape, o...  0.81 us

profile of v4, /device:TPU:0, one launch (start us, length us, event | category | flops | bytes accessed | tf_op | source)
XLA Modules:
  0.0 27.9 jit_solution(13581274789404271519)
XLA Ops:
  1.3 25.8 %shard_map.149 = (bf16[4,512]{1,0:T(4,128)(2,1)S(1)}, f32[8,128,128]{2,1,0:T(8,128)S(1)}) custom-call(bf16[4,1024]{1,0:T(4,128)(2,1)} %refs_0_.1, s32[1,1]{1,0:T(1,128)} %bitcast.7.refs_1_, f32[8,128,128]{2,1,0:T(8,128)} %bitcast.10, bf16[1024,1024]{1,0:T(8,128)(2,1)} %refs_3_.1, bf16[1024,1024]{1,0:T(8,128)(2,1)} %refs_4_.1, bf16[1024,1024]{1,0:T(8,128)(2,1)} %refs_5_.1, ...), custom_call_target="tpu_custom_call" | custom-call | tf_op jit(solution)/shard_map/pallas_call | solution.py:577
  27.1 0.8 %shard_map.150 = (bf16[4,512]{1,0:T(4,128)(2,1)}, f32[8,128,128]{2,1,0:T(8,128)}) custom-call(bf16[4,512]{1,0:T(4,128)(2,1)S(1)} %get-tuple-element.6.out_v, f32[8,128,128]{2,1,0:T(8,128)S(1)} %get-tuple-element.7.nst_v), custom_call_target="tpu_custom_call" | custom-call | tf_op jit(solution)/shard_map/pallas_call | solution.py:609

commit v5 on v4

--- a/solution.py
+++ b/solution.py
@@ -45,7 +45,7 @@
     kv_count,
     tp_count,
     tok_h,
-    pos_h,
+    pos,
     state_h,
     wq_h,
     wk_h,
@@ -61,7 +61,6 @@
     out_v,
     nst,
     tok,
-    pos,
     state,
     wq,
     wk,
@@ -125,12 +124,11 @@
         return copy
 
     tok_load = load(tok_h, tok)
-    pos_load = load(pos_h, pos)
-    inv_load = load(inv_h, inv)
     deep = wg.shape[0] // 2
     halves = [pl.ds(0, deep), pl.ds(deep, deep)]
     proj_loads = [[load(src, dst)] for src, dst in ((wq_h, wq), (wk_h, wk), (wv_h, wv))]
     proj_loads.append([load(wg_h.at[half], wg.at[half]) for half in halves])
+    inv_load = load(inv_h, inv)
     state_load = load(state_h, state)
     gmix_load = load(gmix_h, gmix)
     gout_load = load(gout_h, gout)
@@ -139,20 +137,12 @@
     for chip, core in far_peers + [(kv, core) for core in beside]:
         pl.semaphore_signal(barrier, inc=1, device_id=(dp, chip, core), device_id_type=MESH)
 
-    pos_load.wait()
-    inv_load.wait()
-    lane = lax.broadcasted_iota(jnp.int32, (1, width_head), 1)
     eye[...] = jnp.where(
         lax.broadcasted_iota(jnp.int32, eye.shape, 0)
         == lax.broadcasted_iota(jnp.int32, eye.shape, 1),
         1.0,
         0.0,
     ).astype(BF16)
-    angle = pos[...].astype(F32) * inv[...]
-    cosine = jnp.cos(angle)
-    sine = jnp.sin(angle)
-    sine = jnp.where(lane < width_head // 2, -sine, sine)
-
     tok_load.wait()
     later = []
 
@@ -283,6 +273,13 @@
     lax.fori_loop(0, turns[0], turn, 0)
     for copy in part_copies(3):
         copy.start()
+    inv_load.wait()
+    lane = lax.broadcasted_iota(jnp.int32, (1, width_head), 1)
+    angle = pos[0].astype(F32) * inv[...]
+    cosine = jnp.cos(angle)
+    sine = jnp.sin(angle)
+    sine = jnp.where(lane < width_head // 2, -sine, sine)
+
     lax.fori_loop(turns[0], turns[1], turn, 0)
 
     state_load.wait()
@@ -353,9 +350,6 @@
     for core in beside:
         gate_copy(core).start()
 
-    key_t = jnp.transpose(key)
-    for h in range(heads):
-        nst[h] = decay[h : h + 1, :] * state[h] + key_t[:, h : h + 1] * value[h : h + 1, :]
 
     lax.fori_loop(turns[2], pieces, turn, 0)
 
@@ -423,6 +417,9 @@
                 acc[:, at] = part if first else acc[:, at] + part
 
     own = own - shift
+    key_t = jnp.transpose(key)
+    for h in range(heads):
+        nst[h] = decay[h : h + 1, :] * state[h] + key_t[:, h : h + 1] * value[h : h + 1, :]
     up_part(centred(own, own_lanes), own_lanes, True)
     total = own
     squares = own * own
@@ -556,7 +553,7 @@
     inverse = np.tile(inverse.astype(np.float32), 2)[None, :]
     arrays = (
         tokens,
-        positions[None, :],
+        positions,
         state[0],
         w_query,
         w_key,
@@ -571,7 +568,8 @@
         jnp.asarray(inverse),
     )
     held = [pltpu.VMEM(a.shape, a.dtype) for a in arrays]
-    held[9:11] = [pltpu.VMEM((2, w_ffn_gate.shape[1], width), BF16)]
+    del held[1]
+    held[8:10] = [pltpu.VMEM((2, w_ffn_gate.shape[1], width), BF16)]
     vmem_spec = pl.BlockSpec(memory_space=pltpu.VMEM)
     any_spec = pl.BlockSpec(memory_space=pl.ANY)
     out, new_state = pl.pallas_call(
@@ -580,7 +578,8 @@
             pltpu.VMEM((rows, cols), BF16),
             pltpu.VMEM(state.shape[1:], F32),
         ),
-        in_specs=[any_spec] * len(arrays),
+        in_specs=[any_spec, pl.BlockSpec(memory_space=pltpu.SMEM)]
+        + [any_spec] * (len(arrays) - 2),
         out_specs=(vmem_spec, vmem_spec),
         scratch_shapes=held
         + [

time: 28.1 us -> 28.1 us (level)
  no operation moved by 1% of the time
where the time goes in v5:
time: 28.1 us; the launch traced here: 27.9 us
  Pallas kernels  26.6 us (95%)
  between operations  1.29 us (5%)
    pallas_call x1, Pallas kernels, fused_step(): pl.pallas_call(functools.partial(step_kernel, kv_count, tp_count), out_sh...  25.8 us
    pallas_call x1, Pallas kernels, fused_step(): pl.pallas_call(store_kernel, out_shape=(jax.ShapeDtypeStruct(out.shape, o...  0.81 us

profile of v5, /device:TPU:0, one launch (start us, length us, event | category | flops | bytes accessed | tf_op | source)
XLA Modules:
  0.0 27.9 jit_solution(2998052446129992516)
XLA Ops:
  1.3 25.8 %shard_map.149 = (bf16[4,512]{1,0:T(4,128)(2,1)S(1)}, f32[8,128,128]{2,1,0:T(8,128)S(1)}) custom-call(bf16[4,1024]{1,0:T(4,128)(2,1)} %refs_0_.1, s32[1]{0:T(128)S(6)} %copy.16.refs_1_, f32[8,128,128]{2,1,0:T(8,128)} %bitcast.8, bf16[1024,1024]{1,0:T(8,128)(2,1)} %refs_3_.1, bf16[1024,1024]{1,0:T(8,128)(2,1)} %refs_4_.1, bf16[1024,1024]{1,0:T(8,128)(2,1)} %refs_5_.1, ...), custom_call_target="tpu_custom_call" | custom-call | tf_op jit(solution)/shard_map/pallas_call | solution.py:575
  27.1 0.8 %shard_map.150 = (bf16[4,512]{1,0:T(4,128)(2,1)}, f32[8,128,128]{2,1,0:T(8,128)}) custom-call(bf16[4,512]{1,0:T(4,128)(2,1)S(1)} %get-tuple-element.6.out_v, f32[8,128,128]{2,1,0:T(8,128)S(1)} %get-tuple-element.7.nst_v), custom_call_target="tpu_custom_call" | custom-call | tf_op jit(solution)/shard_map/pallas_call | solution.py:608

commit v6 on v4

--- a/solution.py
+++ b/solution.py
@@ -437,7 +437,7 @@
         order = list(reversed(range(tp_count)))
         if k == kv_count - 2:
             wfd_load.wait()
-        for part in [[core] for core in order] if k in (0,) else [order]:
+        for part in [[core] for core in order] if k in (0, 1) else [order]:
             for core in part:
                 wait_from(1, mix, chip, core)
             blocks = []

time: 28.1 us -> 28.2 us (level)
  no operation moved by 1% of the time
where the time goes in v6:
time: 28.2 us; the launch traced here: 28 us
  Pallas kernels  26.7 us (95%)
  between operations  1.29 us (5%)
    pallas_call x1, Pallas kernels, fused_step(): pl.pallas_call(functools.partial(step_kernel, kv_count, tp_count), out_sh...  25.9 us
    pallas_call x1, Pallas kernels, fused_step(): pl.pallas_call(store_kernel, out_shape=(jax.ShapeDtypeStruct(out.shape, o...  0.81 us

profile of v6, /device:TPU:0, one launch (start us, length us, event | category | flops | bytes accessed | tf_op | source)
XLA Modules:
  0.0 28.0 jit_solution(11612372859682830023)
XLA Ops:
  1.3 25.9 %shard_map.149 = (bf16[4,512]{1,0:T(4,128)(2,1)S(1)}, f32[8,128,128]{2,1,0:T(8,128)S(1)}) custom-call(bf16[4,1024]{1,0:T(4,128)(2,1)} %refs_0_.1, s32[1,1]{1,0:T(1,128)} %bitcast.7.refs_1_, f32[8,128,128]{2,1,0:T(8,128)} %bitcast.10, bf16[1024,1024]{1,0:T(8,128)(2,1)} %refs_3_.1, bf16[1024,1024]{1,0:T(8,128)(2,1)} %refs_4_.1, bf16[1024,1024]{1,0:T(8,128)(2,1)} %refs_5_.1, ...), custom_call_target="tpu_custom_call" | custom-call | tf_op jit(solution)/shard_map/pallas_call | solution.py:577
  27.2 0.8 %shard_map.150 = (bf16[4,512]{1,0:T(4,128)(2,1)}, f32[8,128,128]{2,1,0:T(8,128)}) custom-call(bf16[4,512]{1,0:T(4,128)(2,1)S(1)} %get-tuple-element.6.out_v, f32[8,128,128]{2,1,0:T(8,128)S(1)} %get-tuple-element.7.nst_v), custom_call_target="tpu_custom_call" | custom-call | tf_op jit(solution)/shard_map/pallas_call | solution.py:609
